TPU v7x, 32 devices: a whole 2x2x4 slice. The times are simulated.
32 devices in a mesh: fs: 4 (over y, x), tp: 8 (over z, core).
Axes of the slice: x: 2, y: 2, z: 4, core: 2. Of those that a mesh axis runs over, the one named last changes fastest.
Arguments:
- tokens: bfloat16 [512, 4096], P('fs', 'tp'), may hold values from -6 to 6
- expert_ids: int32 [512, 8], P('fs'), may hold values from 0 to 63, all different within a row; in each aligned block of 128 rows (0 to 127, 128 to 255, ...) at most 32 rows name the same one
- affinity: float32 [512, 8], P('fs'), may hold values from 0.05 to 1
- norm_gain: float32 [4096], P('fs'), may hold values from 0.1 to 1.9
- gate_train: float32 [64, 512, 4096], P(None, 'tp', 'fs'), may hold values from -0.09375 to 0.09375
- up_train: float32 [64, 512, 4096], P(None, 'tp', 'fs'), may hold values from -0.09375 to 0.09375
- down_train: float32 [64, 512, 4096], P(None, 'fs', 'tp'), may hold values from -0.25 to 0.25
- shared_gate_train: float32 [512, 4096], P('tp', 'fs'), may hold values from -0.09375 to 0.09375
- shared_up_train: float32 [512, 4096], P('tp', 'fs'), may hold values from -0.09375 to 0.09375
- shared_down_train: float32 [512, 4096], P('fs', 'tp'), may hold values from -0.25 to 0.25
Outputs:
- mixed: bfloat16 [512, 4096], P('fs', 'tp')
- gate_serve: bfloat16 [64, 512, 4096], P('fs', 'tp')
- up_serve: bfloat16 [64, 512, 4096], P('fs', 'tp')
- down_serve: bfloat16 [64, 512, 4096], P('fs', None, 'tp')
- shared_gate_serve: bfloat16 [512, 4096], P('tp')
- shared_up_serve: bfloat16 [512, 4096], P('tp')
- shared_down_serve: bfloat16 [512, 4096], P(None, 'tp')
Inputs may be any that keep to these rules, and one draw needn't show every extreme that they name: `expert_ids`: each row names 8 different experts. In each aligned block of 128 rows (the tokens of one index of fs) no expert is named by more than 32 rows, a bound that some block reaches.
All inputs are finite; a program needn't handle non-finite values.
Results may differ from a plain program's by a relative error of at most 0.019.
Values may be sent and summed in bfloat16 or wider, within the bound.
A program may use at most 192 MiB of HBM per device.

v0:
```python
import functools

import jax
import jax.numpy as jnp
from jax import lax
from jax.experimental import pallas as pl
from jax.experimental.pallas import tpu as pltpu
from jax.sharding import PartitionSpec as P

MESH = pl.DeviceIdType.MESH

norm_eps = 1e-06
routed_scale = 2.5
vmem_bytes = 66900000


def nt_dot(a, b):
    return lax.dot_general(a, b, (((1,), (1,)), ((), ())), preferred_element_type=jnp.float32)


def silu_mul(acc, scale):
    half = acc.shape[1] // 2
    gate = acc[:, :half] * scale
    up = acc[:, half:] * scale
    return gate / (1.0 + jnp.exp(-gate)) * up


def moe_kernel(cfg, *refs):
    n, ntp, group, slots, cols, ge = cfg
    (ids_ref, aff_ref, gain_ref, tok_ref, gate_ref, up_ref, down_ref, sg_ref, su_ref, sd_ref) = refs[:10]
    (mixed_ref, gout, uout, dout, sgo, suo, sdo) = refs[10:17]
    (idv, affv, gainv, rbuf, rland, routes, x, inv, fbuf, sbuf, dfb, dsb) = refs[17:29]
    (gfb, ufb, sfb, gsb, usb, ssb, hid, hids, acc, own, part, landed) = refs[29:41]
    (isem, lsem, tsem, osem, zs, zr, gss, grs, dss, drs, mss, mrs, hs, hr, qs, qr, cs, cr) = refs[41:]

    me = lax.axis_index("fs")
    tp = lax.axis_index("tp")
    dest = [lax.rem(me + k, n) for k in range(n)]
    origin = [lax.rem(me + n - k, n) for k in range(n)]
    nz = ntp // 2
    partner = tp + 1 - 2 * lax.rem(tp, 2)
    zdest = [lax.rem(tp + 2 * k, ntp) for k in range(nz)]
    zorigin = [lax.rem(tp + ntp - 2 * k, ntp) for k in range(nz)]
    porigin = [lax.rem(partner + ntp - 2 * k, ntp) for k in range(nz)]

    rows = tok_ref.shape[0]
    total_rows = n * rows
    topk = ids_ref.shape[0]
    le, hl, d = gout.shape
    dl = d // n
    hd = down_ref.shape[1]
    hidden = hd * n
    cl = down_ref.shape[2]
    pairs = le // group
    gl = group * hl
    cw = cl // cols
    neg = le // ge
    chunks = cols * neg
    order = list(range(1, n)) + [0]

    def at(first, size):
        return pl.ds(pl.multiple_of(first, size), size)

    def to_fs(k):
        return {"fs": dest[k]}

    smalls = [(sg_ref, gfb, gsb, sgo), (su_ref, ufb, usb, suo), (sd_ref, sfb, ssb, sdo)]
    early = [(ids_ref, idv), (aff_ref, affv), (gain_ref, gainv)] + [(s, f) for s, f, _, _ in smalls]

    def early_load(i):
        return pltpu.make_async_copy(early[i][0], early[i][1], isem.at[i])

    weights = [gate_ref, up_ref]
    wouts = [gout, uout]

    def load(w, j, k):
        return pltpu.make_async_copy(
            weights[w].at[pl.ds(dest[k] * le + j * group, group)], fbuf.at[k], lsem.at[0, k]
        )

    def dload(c, k):
        cb, eg = c // neg, lax.rem(c, neg)
        return pltpu.make_async_copy(
            down_ref.at[pl.ds(dest[k] * le + eg * ge, ge), :, at(cb * cw, cw)], dfb.at[k], lsem.at[1, k]
        )

    def own_tokens():
        return pltpu.make_async_copy(tok_ref, x.at[at(me * rows, rows), at(tp * cl, cl)], osem)

    for i in range(len(early)):
        early_load(i).start()
    for k in order:
        load(0, 0, k).start()
    own_tokens().start()

    barrier = pltpu.get_barrier_semaphore()
    for k in range(1, n):
        pl.semaphore_signal(barrier, inc=1, device_id=to_fs(k), device_id_type=MESH)
    for k in range(1, nz):
        pl.semaphore_signal(barrier, inc=1, device_id={"tp": zdest[k]}, device_id_type=MESH)
    pl.semaphore_signal(barrier, inc=1, device_id={"tp": partner}, device_id_type=MESH)
    pl.semaphore_wait(barrier, n - 1 + nz)

    def token_copy(k, source):
        return pltpu.make_async_remote_copy(
            src_ref=tok_ref,
            dst_ref=x.at[at(source * rows, rows), at(tp * cl, cl)],
            send_sem=tsem.at[0, k],
            recv_sem=tsem.at[1, k],
            device_id=to_fs(k),
            device_id_type=MESH,
        )

    def route_copy(k, source):
        return pltpu.make_async_remote_copy(
            src_ref=rbuf,
            dst_ref=rland.at[source],
            send_sem=tsem.at[2, k],
            recv_sem=tsem.at[3, k],
            device_id=to_fs(k),
            device_id_type=MESH,
        )

    for k in range(1, n):
        token_copy(k, me).start()

    for i in range(3):
        early_load(i).wait()
    affinity = affv[...]
    route = jnp.concatenate(
        [idv[...].astype(jnp.float32), routed_scale * affinity / jnp.sum(affinity, axis=0, keepdims=True)], axis=0
    )
    rbuf[...] = route
    rland[me] = route

    def weight_copy(w, k, slot, j, source):
        return pltpu.make_async_remote_copy(
            src_ref=sbuf.at[w, k - 1, slot],
            dst_ref=wouts[w].at[pl.ds(j * group, group), :, at(source * dl, dl)],
            send_sem=gss.at[w, k - 1, slot],
            recv_sem=grs.at[w, k - 1, j],
            device_id=to_fs(k),
            device_id_type=MESH,
        )

    def produce(j):
        slot = lax.rem(j, slots)
        for w in range(2):
            pending = None
            for k in order:
                load(w, j, k).wait()
                for c in range(group):
                    value = (fbuf[k, c] * gainv[...]).astype(jnp.bfloat16)
                    if k == 0:
                        wouts[w][j * group + c, :, at(me * dl, dl)] = value
                    else:
                        sbuf[w, k - 1, slot, c] = value
                if w == 0:
                    load(1, j, k).start()
                else:

                    @pl.when(j + 1 < pairs)
                    def _():
                        load(0, j + 1, k).start()

                if pending is not None:
                    weight_copy(w, pending, slot, j, me).start()
                pending = k

    def first(j, carry):
        produce(j)
        return carry

    lax.fori_loop(0, slots, first, 0)

    for k in range(1, n):
        route_copy(k, me).start()

    def small_place(i, who):
        ref = smalls[i][3]
        if i == 2:
            return ref.at[at(who * hd, hd), :]
        return ref.at[:, at(who * dl, dl)]

    def small_copy(i, k, source):
        return pltpu.make_async_remote_copy(
            src_ref=smalls[i][2],
            dst_ref=small_place(i, source),
            send_sem=mss.at[i, k - 1],
            recv_sem=mrs.at[i, k - 1],
            device_id=to_fs(k),
            device_id_type=MESH,
        )

    for i in range(3):
        early_load(3 + i).wait()
        value = smalls[i][1][...]
        if i < 2:
            value = value * gainv[...]
        value = value.astype(jnp.bfloat16)
        smalls[i][2][...] = value
        small_place(i, me)[...] = value
    for i in range(3):
        for k in range(1, n):
            small_copy(i, k, me).start()

    def z_copy(view, send, recv, index, slot, to):
        return pltpu.make_async_remote_copy(
            src_ref=view(slot),
            dst_ref=view(slot),
            send_sem=send(index),
            recv_sem=recv(index),
            device_id={"tp": to},
            device_id_type=MESH,
        )

    def z_send(view, send, recv):
        for k in range(1, nz):
            z_copy(view, send, recv, k, tp, zdest[k]).start()
        z_copy(view, send, recv, 0, tp, partner).start()

    def z_relay(view, send, recv):
        for k in range(1, nz):
            z_copy(view, send, recv, k, zorigin[k], zdest[k]).wait_recv()
            z_copy(view, send, recv, nz - 1 + k, zorigin[k], partner).start()

    def z_finish(view, send, recv):
        z_copy(view, send, recv, 0, partner, partner).wait_recv()
        for k in range(1, nz):
            z_copy(view, send, recv, nz - 1 + k, porigin[k], partner).wait_recv()

    def z_sent(view, send, recv):
        for k in range(2 * nz - 1):
            z_copy(view, send, recv, k, tp, partner).wait_send()

    def pick(sems):
        return lambda i: sems.at[i]

    def token_view(slot):
        return x.at[:, at(slot * cl, cl)]

    own_tokens().wait()
    for k in range(1, n):
        token_copy(k, origin[k]).wait_recv()
    z_send(token_view, pick(zs), pick(zr))
    for k in range(1, n):
        route_copy(k, origin[k]).wait_recv()
    for f in range(n):
        routes[f * rows : (f + 1) * rows, : 2 * topk] = rland[f].T
    z_relay(token_view, pick(zs), pick(zr))
    z_finish(token_view, pick(zs), pick(zr))

    block = min(512, total_rows)

    def norms(i, carry):
        part_rows = at(i * 128, 128)
        sums = jnp.zeros((128, 1), jnp.float32)
        for c in range(0, d, 512):
            v = x[part_rows, c : c + 512].astype(jnp.float32)
            sums = sums + jnp.sum(v * v, axis=1, keepdims=True)
        inv[part_rows, :] = jnp.broadcast_to(lax.rsqrt(sums / d + norm_eps), (128, inv.shape[1]))
        return carry

    lax.fori_loop(0, total_rows // 128, norms, 0)

    def down_place(c, who):
        cb, eg = c // neg, lax.rem(c, neg)
        return dout.at[pl.ds(eg * ge, ge), at(who * hd, hd), at(cb * cw, cw)]

    def down_copy(k, c, source):
        return pltpu.make_async_remote_copy(
            src_ref=dsb.at[k - 1, c],
            dst_ref=down_place(c, source),
            send_sem=dss.at[k - 1, c],
            recv_sem=drs.at[k - 1, c],
            device_id=to_fs(k),
            device_id_type=MESH,
        )

    def produce_down():
        for k in order:
            dload(0, k).start()

        def step(c, carry):
            pending = None
            for k in order:
                dload(c, k).wait()
                for e in range(ge):
                    value = dfb[k, e].astype(jnp.bfloat16)
                    if k == 0:
                        cb, eg = c // neg, lax.rem(c, neg)
                        dout[eg * ge + e, at(me * hd, hd), at(cb * cw, cw)] = value
                    else:
                        dsb[k - 1, c, e] = value

                @pl.when(c + 1 < chunks)
                def _():
                    dload(c + 1, k).start()

                if pending is not None:
                    down_copy(pending, c, me).start()
                pending = k
            return carry

        lax.fori_loop(0, chunks, step, 0)

    def hid_view(i):
        return lambda slot: hid.at[slot, i]

    def hid_sem(sems, i):
        return lambda k: sems.at[i, k]

    def hid_args(i):
        return hid_view(i), hid_sem(hs, i), hid_sem(hr, i)

    def consume(i, carry):
        for w in range(2):
            for k in range(1, n):
                weight_copy(w, k, 0, i, origin[k]).wait_recv()
        w_all = jnp.concatenate(
            [gout[pl.ds(i * group, group)].reshape(gl, d), uout[pl.ds(i * group, group)].reshape(gl, d)], axis=0
        )

        def rows_step(r, c):
            rs = at(r * block, block)
            h = silu_mul(nt_dot(x[rs, :], w_all), inv[rs, :gl])
            lane = lax.broadcasted_iota(jnp.int32, h.shape, 1)
            expert = (me * le + group * i + lane // hl).astype(jnp.float32)
            weight = jnp.zeros(h.shape, jnp.float32)
            for k in range(topk):
                weight = weight + jnp.where(
                    routes[rs, k : k + 1] == expert, routes[rs, topk + k : topk + k + 1], 0.0
                )
            hid[tp, i, rs, :] = (h * weight).astype(jnp.bfloat16)
            return c

        if total_rows == block:
            rows_step(0, 0)
        else:
            lax.fori_loop(0, total_rows // block, rows_step, 0)

        @pl.when(i > 0)
        def _():
            z_relay(*hid_args(i - 1))

        z_send(*hid_args(i))

        @pl.when(i + slots < pairs)
        def _():
            for w in range(2):
                for k in range(1, n):
                    weight_copy(w, k, lax.rem(i, slots), i, me).wait_send()
            produce(i + slots)

        if pairs > slots:

            @pl.when(i == pairs - slots - 1)
            def _():
                produce_down()

        return carry

    if pairs == slots:
        produce_down()
    lax.fori_loop(0, pairs, consume, 0)
    z_relay(*hid_args(pairs - 1))

    def shared_view(slot):
        return hids.at[slot]

    shared_args = (shared_view, pick(qs), pick(qr))
    for i in range(3):
        for k in range(1, n):
            small_copy(i, k, origin[k]).wait_recv()
    mine = at(me * rows, rows)
    h = silu_mul(nt_dot(x[mine, :], jnp.concatenate([sgo[...], suo[...]], axis=0)), inv[mine, :hl])
    wide = jnp.concatenate([h] * group, axis=1)
    lane = lax.broadcasted_iota(jnp.int32, wide.shape, 1)
    hids[tp] = jnp.where(lane // hl == lax.rem(tp, group), wide, 0.0).astype(jnp.bfloat16)

    def finish(i, carry):
        z_finish(*hid_args(i))
        return carry

    lax.fori_loop(0, pairs, finish, 0)
    z_send(*shared_args)
    z_relay(*shared_args)
    z_finish(*shared_args)
    blocks = []
    for q in range(ntp // group):
        blocks.append(functools.reduce(jnp.add, [hids[q * group + g] for g in range(group)]))
    shared = jnp.dot(jnp.concatenate(blocks, axis=1), sdo[...], preferred_element_type=jnp.float32)
    for cb in range(cols):
        own[cb] = shared[:, cb * cw : (cb + 1) * cw]

    def part_copy(k, cb, who):
        return pltpu.make_async_remote_copy(
            src_ref=part.at[cb, at(who * rows, rows)],
            dst_ref=landed.at[cb, k - 1],
            send_sem=cs.at[cb, k - 1],
            recv_sem=cr.at[cb, k - 1],
            device_id=to_fs(k),
            device_id_type=MESH,
        )

    per = ge // group

    def down_step(c, carry):
        cb, eg = c // neg, lax.rem(c, neg)
        for k in range(1, n):
            down_copy(k, c, origin[k]).wait_recv()
        left, right = [], []
        for p in range(per):
            pair = eg * per + p
            for s in range(ntp):
                left.append(hid.at[s, pair])
                right.append(
                    dout[pl.ds(pair * group, group), s * hl : (s + 1) * hl, at(cb * cw, cw)].reshape(gl, cw)
                )
        down = jnp.concatenate(right, axis=0)

        def rows_step(r, q):
            rs = at(r * block, block)
            lhs = jnp.concatenate([ref[rs, :] for ref in left], axis=1)
            total = jnp.dot(lhs, down, preferred_element_type=jnp.float32)

            @pl.when(eg == 0)
            def _():
                acc[rs, :] = total

            @pl.when(eg > 0)
            def _():
                acc[rs, :] += total

            return q

        if total_rows == block:
            rows_step(0, 0)
        else:
            lax.fori_loop(0, total_rows // block, rows_step, 0)

        @pl.when(eg == neg - 1)
        def _():
            part[cb] = acc[...].astype(jnp.bfloat16)
            own[cb] += acc[mine, :]
            for k in range(1, n):
                part_copy(k, cb, dest[k]).start()

        return carry

    lax.fori_loop(0, chunks, down_step, 0)

    for k in range(1, n):
        token_copy(k, me).wait_send()
        route_copy(k, me).wait_send()
        for i in range(3):
            small_copy(i, k, me).wait_send()
    z_sent(token_view, pick(zs), pick(zr))
    z_sent(*shared_args)

    def sent(i, carry):
        z_sent(*hid_args(i))
        return carry

    lax.fori_loop(0, pairs, sent, 0)

    def weights_sent(j, carry):
        for w in range(2):
            for k in range(1, n):
                weight_copy(w, k, lax.rem(j, slots), j, me).wait_send()
        return carry

    lax.fori_loop(pairs - slots, pairs, weights_sent, 0)

    def down_sent(c, carry):
        for k in range(1, n):
            down_copy(k, c, me).wait_send()
        return carry

    lax.fori_loop(0, chunks, down_sent, 0)

    for cb in range(cols):
        result = own[cb]
        for k in range(1, n):
            part_copy(k, cb, dest[k]).wait()
            result = result + landed[cb, k - 1].astype(jnp.float32)
        mixed_ref[:, cb * cw : (cb + 1) * cw] = result.astype(mixed_ref.dtype)


def moe_call(n, ntp, args):
    ids, aff, gain, tokens, gate, up, down, sg, su, sd = args
    bf16, f32 = jnp.bfloat16, jnp.float32
    experts, hl, dl = gate.shape
    _, hd, cl = down.shape
    rows = tokens.shape[0]
    topk = ids.shape[0]
    le, d, hidden, total = experts // n, dl * n, hd * n, rows * n
    group = min(le, max(1, 128 // hl))
    pairs = le // group
    slots = min(4, pairs)
    cols = 2 if cl % 256 == 0 else 1
    cw = cl // cols
    ge = group * (2 if pairs % 2 == 0 else 1)
    chunks = cols * (le // ge)
    gl = group * hl
    nz = ntp // 2
    vm, dma = pltpu.VMEM, pltpu.SemaphoreType.DMA
    outs = [
        ((rows, cl), bf16),
        ((le, hl, d), bf16),
        ((le, hl, d), bf16),
        ((le, hidden, cl), bf16),
        ((hl, d), bf16),
        ((hl, d), bf16),
        ((hidden, cl), bf16),
    ]
    pinned = sum(functools.reduce(lambda a, b: a * b, s) * 2 for s, _ in outs)
    hbm = pl.BlockSpec(memory_space=pltpu.HBM)
    args = [pltpu.with_memory_space_constraint(a, pltpu.HBM) for a in args]
    results = pl.pallas_call(
        functools.partial(moe_kernel, (n, ntp, group, slots, cols, ge)),
        out_shape=tuple(vm(s, t) for s, t in outs),
        in_specs=[hbm] * len(args),
        out_specs=(pl.BlockSpec(memory_space=vm),) * len(outs),
        scratch_shapes=[
            vm(ids.shape, ids.dtype),
            vm(aff.shape, f32),
            vm(gain.shape, f32),
            vm((2 * topk, rows), f32),
            vm((n, 2 * topk, rows), f32),
            vm((total, 128), f32),
            vm((total, d), bf16),
            vm((total, 128), f32),
            vm((n, group, hl, dl), f32),
            vm((2, n - 1, slots, group, hl, dl), bf16),
            vm((n, ge, hd, cw), f32),
            vm((n - 1, chunks, ge, hd, cw), bf16),
            vm(sg.shape, f32),
            vm(su.shape, f32),
            vm(sd.shape, f32),
            vm(sg.shape, bf16),
            vm(su.shape, bf16),
            vm(sd.shape, bf16),
            vm((ntp, pairs, total, gl), bf16),
            vm((ntp, rows, gl), bf16),
            vm((total, cw), f32),
            vm((cols, rows, cw), f32),
            vm((cols, total, cw), bf16),
            vm((cols, n - 1, rows, cw), bf16),
            dma((6,)),
            dma((2, n)),
            dma((4, n)),
            dma,
            dma((2 * nz - 1,)),
            dma((2 * nz - 1,)),
            dma((2, n - 1, slots)),
            dma((2, n - 1, pairs)),
            dma((n - 1, chunks)),
            dma((n - 1, chunks)),
            dma((3, n - 1)),
            dma((3, n - 1)),
            dma((pairs, 2 * nz - 1)),
            dma((pairs, 2 * nz - 1)),
            dma((2 * nz - 1,)),
            dma((2 * nz - 1,)),
            dma((cols, n - 1)),
            dma((cols, n - 1)),
        ],
        compiler_params=pltpu.CompilerParams(
            collective_id=0, has_side_effects=True, vmem_limit_bytes=min(60 * 1024 * 1024, vmem_bytes - pinned)
        ),
        cost_estimate=pl.CostEstimate(flops=6 * total * d * hl * le, bytes_accessed=40 * gate.size, transcendentals=0),
    )(*args)

    def write(*refs):
        count = len(outs)
        sem = refs[-1]
        copies = [pltpu.make_async_copy(refs[i], refs[count + i], sem.at[i]) for i in range(count)]
        for c in copies:
            c.start()
        for c in copies:
            c.wait()

    return pl.pallas_call(
        write,
        out_shape=tuple(jax.ShapeDtypeStruct(s, t) for s, t in outs),
        in_specs=[pl.BlockSpec(memory_space=vm)] * len(outs),
        out_specs=(hbm,) * len(outs),
        scratch_shapes=[dma((len(outs),))],
        compiler_params=pltpu.CompilerParams(vmem_limit_bytes=1024 * 1024),
        cost_estimate=pl.CostEstimate(flops=0, bytes_accessed=pinned, transcendentals=0),
    )(*results)


def body(
    n,
    ntp,
    tokens,
    expert_ids,
    affinity,
    norm_gain,
    gate_train,
    up_train,
    down_train,
    shared_gate_train,
    shared_up_train,
    shared_down_train,
):
    return moe_call(
        n,
        ntp,
        [
            expert_ids.T,
            affinity.T,
            norm_gain[None, :],
            tokens,
            gate_train,
            up_train,
            down_train,
            shared_gate_train,
            shared_up_train,
            shared_down_train,
        ],
    )


def solution(mesh):
    return jax.shard_map(
        functools.partial(body, mesh.shape["fs"], mesh.shape["tp"]),
        mesh=mesh,
        in_specs=(
            P("fs", "tp"),
            P("fs", None),
            P("fs", None),
            P("fs"),
            P(None, "tp", "fs"),
            P(None, "tp", "fs"),
            P(None, "fs", "tp"),
            P("tp", "fs"),
            P("tp", "fs"),
            P("fs", "tp"),
        ),
        out_specs=(
            P("fs", "tp"),
            P("fs", "tp", None),
            P("fs", "tp", None),
            P("fs", None, "tp"),
            P("tp", None),
            P("tp", None),
            P(None, "tp"),
        ),
        check_vma=False,
    )
```

profile of v0, /device:TPU:0, one launch (start us, length us, event | category | flops | bytes accessed | tf_op | source)
XLA Modules:
  0.0 319.7 jit_solution(10046884675954511545)
XLA Ops:
  0.6 310.0 %shard_map.153 = (bf16[128,512]{1,0:T(8,128)(2,1)S(1)}, bf16[16,64,4096]{2,1,0:T(8,128)(2,1)S(1)}, bf16[16,64,4096]{2,1,0:T(8,128)(2,1)S(1)}, bf16[16,512,512]{2...) custom-call(s32[8,128]{1,0:T(8,128)} %bitcast.3, ...), custom_call_target="tpu_custom_call" | custom-call | flops 12884901888 | bytes 167772160 | tf_op jit(solution)/shard_map/pallas_call | solution.py:520
  310.7 9.0 %shard_map.154 = (bf16[128,512]{1,0:T(8,128)(2,1)}, bf16[16,64,4096]{2,1,0:T(8,128)(2,1)}, bf16[16,64,4096]{2,1,0:T(8,128)(2,1)}, bf16[16,512,512]{2,1,0:T(8,128...) custom-call(bf16[128,512]{1,0:T(8,128)(2,1)S(1)} %get-tuple-element.14.refs_0_, ...), custom_call_target="tpu_custom_call" | custom-call | bytes 26869760 | tf_op jit(solution)/shard_map/pallas_call | solution.py:584
where the time goes:
time: 320 us
  Pallas kernels  319 us (100%)
    pallas_call x1, Pallas kernels, moe_call(): pl.pallas_call(functools.partial(moe_kernel, (n, ntp, group, slots, cols,...  310 us
    pallas_call x1, Pallas kernels, moe_call(): pl.pallas_call(write, out_shape=tuple((jax.ShapeDtypeStruct(s, t) for s,...  9.02 us

commit v1 on v0

--- a/solution.py
+++ b/solution.py
@@ -18,6 +18,24 @@
     return lax.dot_general(a, b, (((1,), (1,)), ((), ())), preferred_element_type=jnp.float32)
 
 
+def mate(me, k, n):
+    if n & (n - 1):
+        return lax.rem(me + k, n)
+    other, bit = 0, 1
+    while bit < n:
+        other = other + bit * lax.rem(lax.div(me, bit) + k // bit, 2)
+        bit *= 2
+    return other
+
+
+def mate_origin(me, k, n):
+    return lax.rem(me + n - k, n) if n & (n - 1) else mate(me, k, n)
+
+
+def mate_pairs(k, n):
+    return [(i, (i + k) % n if n & (n - 1) else i ^ k) for i in range(n)]
+
+
 def silu_mul(acc, scale):
     half = acc.shape[1] // 2
     gate = acc[:, :half] * scale
@@ -28,10 +46,12 @@
 def moe_kernel(cfg, *refs):
     n, ntp, group, slots, cols, ge = cfg
     (ids_ref, aff_ref, gain_ref, tok_ref, gate_ref, up_ref, down_ref, sg_ref, su_ref, sd_ref) = refs[:10]
-    (mixed_ref, gout, uout, dout, sgo, suo, sdo) = refs[10:17]
-    (idv, affv, gainv, rbuf, rland, routes, x, inv, fbuf, sbuf, dfb, dsb) = refs[17:29]
-    (gfb, ufb, sfb, gsb, usb, ssb, hid, hids, acc, own, part, landed) = refs[29:41]
-    (isem, lsem, tsem, osem, zs, zr, gss, grs, dss, drs, mss, mrs, hs, hr, qs, qr, cs, cr) = refs[41:]
+    (gout, uout, dout, sgo, suo, own) = refs[10:16]
+    lasts = refs[16 : 15 + n]
+    refs = refs[15 + n :]
+    (idv, affv, gainv, rbuf, rland, routes, x, inv, fbuf, sbuf, dfb, dsb) = refs[:12]
+    (gfb, ufb, sfb, ssb, hid, acc, part, landed) = refs[12:20]
+    (isem, lsem, tsem, osem, zs, zr, gss, grs, dss, drs, mss, mrs, hs, hr, cs, cr, rsem) = refs[20:]
 
     me = lax.axis_index("fs")
     tp = lax.axis_index("tp")
@@ -49,7 +69,7 @@
     le, hl, d = gout.shape
     dl = d // n
     hd = down_ref.shape[1]
-    hidden = hd * n
+    sources = hd // hl
     cl = down_ref.shape[2]
     pairs = le // group
     gl = group * hl
@@ -64,8 +84,8 @@
     def to_fs(k):
         return {"fs": dest[k]}
 
-    smalls = [(sg_ref, gfb, gsb, sgo), (su_ref, ufb, usb, suo), (sd_ref, sfb, ssb, sdo)]
-    early = [(ids_ref, idv), (aff_ref, affv), (gain_ref, gainv)] + [(s, f) for s, f, _, _ in smalls]
+    smalls = [(gfb, sgo), (ufb, suo)]
+    early = [(ids_ref, idv), (aff_ref, affv), (gain_ref, gainv), (sg_ref, gfb), (su_ref, ufb), (sd_ref, sfb)]
 
     def early_load(i):
         return pltpu.make_async_copy(early[i][0], early[i][1], isem.at[i])
@@ -101,28 +121,68 @@
     pl.semaphore_signal(barrier, inc=1, device_id={"tp": partner}, device_id_type=MESH)
     pl.semaphore_wait(barrier, n - 1 + nz)
 
-    def token_copy(k, source):
+    relay = n == 4
+    near = [mate(me, k, n) for k in (1, 2)] if relay else []
+    far = mate(me, 3, n) if relay else None
+
+    def fs_copy(src, dst, sems, index, to):
         return pltpu.make_async_remote_copy(
-            src_ref=tok_ref,
-            dst_ref=x.at[at(source * rows, rows), at(tp * cl, cl)],
-            send_sem=tsem.at[0, k],
-            recv_sem=tsem.at[1, k],
-            device_id=to_fs(k),
+            src_ref=src,
+            dst_ref=dst,
+            send_sem=sems[0](index),
+            recv_sem=sems[1](index),
+            device_id={"fs": to},
             device_id_type=MESH,
         )
+
+    def gather_start(src, view, sems):
+        for i, to in enumerate(near if relay else dest[1:]):
+            fs_copy(src, view(me, None), sems, i, to).start()
+
+    def gather_relay(view, sems):
+        if relay:
+            for i in range(2):
+                whole = view(near[i], None)
+                fs_copy(whole, whole, sems, i, near[i]).wait_recv()
+                half = view(near[i], i)
+                fs_copy(half, half, sems, 2 + i, near[1 - i]).start()
+
+    def gather_wait(view, sems):
+        if relay:
+            for i in range(2):
+                half = view(far, i)
+                fs_copy(half, half, sems, 2 + i, near[1 - i]).wait_recv()
+        else:
+            for k in range(1, n):
+                whole = view(origin[k], None)
+                fs_copy(whole, whole, sems, k - 1, dest[k]).wait_recv()
+
+    def gather_sent(view, sems):
+        for i in range(2 if relay else n - 1):
+            whole = view(me, None)
+            fs_copy(whole, whole, sems, i, dest[1]).wait_send()
+        if relay:
+            for i in range(2):
+                half = view(near[i], i)
+                fs_copy(half, half, sems, 2 + i, near[1 - i]).wait_send()
+
+    def token_place(who, half):
+        size = rows if half is None else rows // 2
+        return x.at[at(who * rows + (half or 0) * size, size), at(tp * cl, cl)]
+
+    token_sems = (lambda i: tsem.at[0, i], lambda i: tsem.at[1, i])
 
     def route_copy(k, source):
         return pltpu.make_async_remote_copy(
             src_ref=rbuf,
             dst_ref=rland.at[source],
-            send_sem=tsem.at[2, k],
-            recv_sem=tsem.at[3, k],
+            send_sem=rsem.at[0, k],
+            recv_sem=rsem.at[1, k],
             device_id=to_fs(k),
             device_id_type=MESH,
         )
 
-    for k in range(1, n):
-        token_copy(k, me).start()
+    gather_start(tok_ref, token_place, token_sems)
 
     for i in range(3):
         early_load(i).wait()
@@ -169,6 +229,11 @@
 
     def first(j, carry):
         produce(j)
+
+        @pl.when(j == 0)
+        def _():
+            gather_relay(token_place, token_sems)
+
         return carry
 
     lax.fori_loop(0, slots, first, 0)
@@ -176,33 +241,21 @@
     for k in range(1, n):
         route_copy(k, me).start()
 
-    def small_place(i, who):
-        ref = smalls[i][3]
-        if i == 2:
-            return ref.at[at(who * hd, hd), :]
-        return ref.at[:, at(who * dl, dl)]
-
-    def small_copy(i, k, source):
-        return pltpu.make_async_remote_copy(
-            src_ref=smalls[i][2],
-            dst_ref=small_place(i, source),
-            send_sem=mss.at[i, k - 1],
-            recv_sem=mrs.at[i, k - 1],
-            device_id=to_fs(k),
-            device_id_type=MESH,
-        )
-
-    for i in range(3):
+    def small_place(i):
+        def view(who, half):
+            size = hl if half is None else hl // 2
+            return smalls[i][1].at[pl.ds((half or 0) * size, size), at(who * dl, dl)]
+
+        return view
+
+    small_sems = [(lambda k, i=i: mss.at[i, k], lambda k, i=i: mrs.at[i, k]) for i in range(2)]
+    for i in range(2):
         early_load(3 + i).wait()
-        value = smalls[i][1][...]
-        if i < 2:
-            value = value * gainv[...]
-        value = value.astype(jnp.bfloat16)
-        smalls[i][2][...] = value
-        small_place(i, me)[...] = value
-    for i in range(3):
-        for k in range(1, n):
-            small_copy(i, k, me).start()
+        smalls[i][1][:, at(me * dl, dl)] = (smalls[i][0][...] * gainv[...]).astype(jnp.bfloat16)
+    for i in range(2):
+        gather_start(small_place(i)(me, None), small_place(i), small_sems[i])
+    early_load(5).wait()
+    ssb[...] = sfb[...].astype(jnp.bfloat16)
 
     def z_copy(view, send, recv, index, slot, to):
         return pltpu.make_async_remote_copy(
@@ -240,8 +293,7 @@
         return x.at[:, at(slot * cl, cl)]
 
     own_tokens().wait()
-    for k in range(1, n):
-        token_copy(k, origin[k]).wait_recv()
+    gather_wait(token_place, token_sems)
     z_send(token_view, pick(zs), pick(zr))
     for k in range(1, n):
         route_copy(k, origin[k]).wait_recv()
@@ -345,6 +397,13 @@
 
         z_send(*hid_args(i))
 
+        if pairs > slots:
+
+            @pl.when(i == pairs - slots - 1)
+            def _():
+                for q in range(2):
+                    gather_relay(small_place(q), small_sems[q])
+
         @pl.when(i + slots < pairs)
         def _():
             for w in range(2):
@@ -361,37 +420,37 @@
         return carry
 
     if pairs == slots:
+        for q in range(2):
+            gather_relay(small_place(q), small_sems[q])
         produce_down()
     lax.fori_loop(0, pairs, consume, 0)
     z_relay(*hid_args(pairs - 1))
 
-    def shared_view(slot):
-        return hids.at[slot]
-
-    shared_args = (shared_view, pick(qs), pick(qr))
-    for i in range(3):
-        for k in range(1, n):
-            small_copy(i, k, origin[k]).wait_recv()
-    mine = at(me * rows, rows)
-    h = silu_mul(nt_dot(x[mine, :], jnp.concatenate([sgo[...], suo[...]], axis=0)), inv[mine, :hl])
-    wide = jnp.concatenate([h] * group, axis=1)
-    lane = lax.broadcasted_iota(jnp.int32, wide.shape, 1)
-    hids[tp] = jnp.where(lane // hl == lax.rem(tp, group), wide, 0.0).astype(jnp.bfloat16)
+    for i in range(2):
+        gather_wait(small_place(i), small_sems[i])
+    shared_all = jnp.concatenate([sgo[...], suo[...]], axis=0)
+
+    def shared_step(r, c):
+        rs = at(r * block, block)
+        h = silu_mul(nt_dot(x[rs, :], shared_all), inv[rs, :hl])
+        wide = jnp.concatenate([h] * group, axis=1)
+        lane = lax.broadcasted_iota(jnp.int32, wide.shape, 1)
+        hid[tp, pairs, rs, :] = jnp.where(lane // hl == lax.rem(tp, sources), wide, 0.0).astype(jnp.bfloat16)
+        return c
+
+    if total_rows == block:
+        shared_step(0, 0)
+    else:
+        lax.fori_loop(0, total_rows // block, shared_step, 0)
+    z_send(*hid_args(pairs))
 
     def finish(i, carry):
         z_finish(*hid_args(i))
         return carry
 
     lax.fori_loop(0, pairs, finish, 0)
-    z_send(*shared_args)
-    z_relay(*shared_args)
-    z_finish(*shared_args)
-    blocks = []
-    for q in range(ntp // group):
-        blocks.append(functools.reduce(jnp.add, [hids[q * group + g] for g in range(group)]))
-    shared = jnp.dot(jnp.concatenate(blocks, axis=1), sdo[...], preferred_element_type=jnp.float32)
-    for cb in range(cols):
-        own[cb] = shared[:, cb * cw : (cb + 1) * cw]
+    z_relay(*hid_args(pairs))
+    z_finish(*hid_args(pairs))
 
     def part_copy(k, cb, who):
         return pltpu.make_async_remote_copy(
@@ -404,6 +463,7 @@
         )
 
     per = ge // group
+    mine = at(me * rows, rows)
 
     def down_step(c, carry):
         cb, eg = c // neg, lax.rem(c, neg)
@@ -426,7 +486,9 @@
 
             @pl.when(eg == 0)
             def _():
-                acc[rs, :] = total
+                units = functools.reduce(jnp.add, [hid[me * sources + q, pairs, rs, :hd] for q in range(sources)])
+                shared = jnp.dot(units, ssb[:, at(cb * cw, cw)], preferred_element_type=jnp.float32)
+                acc[rs, :] = total + shared
 
             @pl.when(eg > 0)
             def _():
@@ -439,30 +501,38 @@
         else:
             lax.fori_loop(0, total_rows // block, rows_step, 0)
 
-        @pl.when(eg == neg - 1)
-        def _():
-            part[cb] = acc[...].astype(jnp.bfloat16)
-            own[cb] += acc[mine, :]
-            for k in range(1, n):
-                part_copy(k, cb, dest[k]).start()
+        if cols > 1:
+
+            @pl.when((eg == neg - 1) & (cb < cols - 1))
+            def _():
+                part[cb] = acc[...].astype(jnp.bfloat16)
+                own[:, at(cb * cw, cw)] = acc[mine, :]
+                for k in range(1, n):
+                    part_copy(k, cb, dest[k]).start()
 
         return carry
 
     lax.fori_loop(0, chunks, down_step, 0)
-
+    fold = rows // cols
     for k in range(1, n):
-        token_copy(k, me).wait_send()
+        to = mate(me, k, n)
+        lasts[k - 1][:hd, :] = ssb[...]
+        for c in range(cols):
+            lasts[k - 1][hd:, c * cw : (c + 1) * cw] = acc[at(to * rows + c * fold, fold), :].astype(jnp.bfloat16)
+    own[:, cl - cw :] = acc[mine, :]
+
+    for k in range(1, n):
         route_copy(k, me).wait_send()
-        for i in range(3):
-            small_copy(i, k, me).wait_send()
+    gather_sent(token_place, token_sems)
+    for i in range(2):
+        gather_sent(small_place(i), small_sems[i])
     z_sent(token_view, pick(zs), pick(zr))
-    z_sent(*shared_args)
 
     def sent(i, carry):
         z_sent(*hid_args(i))
         return carry
 
-    lax.fori_loop(0, pairs, sent, 0)
+    lax.fori_loop(0, pairs + 1, sent, 0)
 
     def weights_sent(j, carry):
         for w in range(2):
@@ -479,12 +549,12 @@
 
     lax.fori_loop(0, chunks, down_sent, 0)
 
-    for cb in range(cols):
-        result = own[cb]
+    for cb in range(cols - 1):
+        result = own[:, cb * cw : (cb + 1) * cw]
         for k in range(1, n):
             part_copy(k, cb, dest[k]).wait()
             result = result + landed[cb, k - 1].astype(jnp.float32)
-        mixed_ref[:, cb * cw : (cb + 1) * cw] = result.astype(mixed_ref.dtype)
+        own[:, cb * cw : (cb + 1) * cw] = result
 
 
 def moe_call(n, ntp, args):
@@ -499,22 +569,15 @@
     pairs = le // group
     slots = min(4, pairs)
     cols = 2 if cl % 256 == 0 else 1
-    cw = cl // cols
+    cw, early = cl // cols, max(1, cols - 1)
     ge = group * (2 if pairs % 2 == 0 else 1)
     chunks = cols * (le // ge)
     gl = group * hl
     nz = ntp // 2
     vm, dma = pltpu.VMEM, pltpu.SemaphoreType.DMA
-    outs = [
-        ((rows, cl), bf16),
-        ((le, hl, d), bf16),
-        ((le, hl, d), bf16),
-        ((le, hidden, cl), bf16),
-        ((hl, d), bf16),
-        ((hl, d), bf16),
-        ((hidden, cl), bf16),
-    ]
-    pinned = sum(functools.reduce(lambda a, b: a * b, s) * 2 for s, _ in outs)
+    serve = [((le, hl, d), bf16), ((le, hl, d), bf16), ((le, hidden, cl), bf16), ((hl, d), bf16), ((hl, d), bf16)]
+    outs = serve + [((rows, cl), f32)] + [((hd + rows // cols, cl), bf16)] * (n - 1)
+    pinned = sum(functools.reduce(lambda a, b: a * b, s) * jnp.dtype(t).itemsize for s, t in outs)
     hbm = pl.BlockSpec(memory_space=pltpu.HBM)
     args = [pltpu.with_memory_space_constraint(a, pltpu.HBM) for a in args]
     results = pl.pallas_call(
@@ -538,18 +601,14 @@
             vm(sg.shape, f32),
             vm(su.shape, f32),
             vm(sd.shape, f32),
-            vm(sg.shape, bf16),
-            vm(su.shape, bf16),
             vm(sd.shape, bf16),
-            vm((ntp, pairs, total, gl), bf16),
-            vm((ntp, rows, gl), bf16),
+            vm((ntp, pairs + 1, total, gl), bf16),
             vm((total, cw), f32),
-            vm((cols, rows, cw), f32),
-            vm((cols, total, cw), bf16),
-            vm((cols, n - 1, rows, cw), bf16),
+            vm((early, total, cw), bf16),
+            vm((early, n - 1, rows, cw), bf16),
             dma((6,)),
             dma((2, n)),
-            dma((4, n)),
+            dma((2, max(4, n))),
             dma,
             dma((2 * nz - 1,)),
             dma((2 * nz - 1,)),
@@ -557,14 +616,13 @@
             dma((2, n - 1, pairs)),
             dma((n - 1, chunks)),
             dma((n - 1, chunks)),
-            dma((3, n - 1)),
-            dma((3, n - 1)),
-            dma((pairs, 2 * nz - 1)),
-            dma((pairs, 2 * nz - 1)),
-            dma((2 * nz - 1,)),
-            dma((2 * nz - 1,)),
-            dma((cols, n - 1)),
-            dma((cols, n - 1)),
+            dma((2, max(4, n))),
+            dma((2, max(4, n))),
+            dma((pairs + 1, 2 * nz - 1)),
+            dma((pairs + 1, 2 * nz - 1)),
+            dma((early, n - 1)),
+            dma((early, n - 1)),
+            dma((2, n)),
         ],
         compiler_params=pltpu.CompilerParams(
             collective_id=0, has_side_effects=True, vmem_limit_bytes=min(60 * 1024 * 1024, vmem_bytes - pinned)
@@ -572,24 +630,77 @@
         cost_estimate=pl.CostEstimate(flops=6 * total * d * hl * le, bytes_accessed=40 * gate.size, transcendentals=0),
     )(*args)
 
+    cut = min(4, le)
+
     def write(*refs):
-        count = len(outs)
+        count = len(serve)
         sem = refs[-1]
-        copies = [pltpu.make_async_copy(refs[i], refs[count + i], sem.at[i]) for i in range(count)]
+        copies = []
+        for i in range(count):
+            step = refs[i].shape[0] // cut
+            for c in range(cut):
+                piece = pl.ds(c * step, step)
+                copies.append(pltpu.make_async_copy(refs[i].at[piece], refs[count + i].at[piece], sem.at[i, c]))
         for c in copies:
             c.start()
         for c in copies:
             c.wait()
 
+    own, sent = results[len(serve)], results[len(serve) + 1 :]
+    moved = [lax.ppermute(sent[k - 1], "fs", mate_pairs(k, n)) for k in range(1, n)]
+    written = pl.pallas_call(
+        write,
+        out_shape=tuple(jax.ShapeDtypeStruct(s, t) for s, t in serve),
+        in_specs=[pl.BlockSpec(memory_space=vm)] * len(serve),
+        out_specs=(hbm,) * len(serve),
+        scratch_shapes=[dma((len(serve), cut))],
+        compiler_params=pltpu.CompilerParams(vmem_limit_bytes=1024 * 1024),
+        cost_estimate=pl.CostEstimate(flops=0, bytes_accessed=10 * pinned, transcendentals=0),
+    )(*results[: len(serve)])
+    mixed, shared_down = finish_call(n, hd, own, sent[0], moved)
+    return (mixed, *written, shared_down)
+
+
+def finish_kernel(n, hd, own, *refs):
+    pieces = refs[:n]
+    mixed_ref, down_ref, sem = refs[n:]
+    me = lax.axis_index("fs")
+    copies = []
+    for k in range(n):
+        source = mate_origin(me, k, n)
+        place = down_ref.at[pl.ds(pl.multiple_of(source * hd, hd), hd)]
+        copies.append(pltpu.make_async_copy(pieces[k].at[pl.ds(0, hd)], place, sem.at[k]))
+        copies[-1].start()
+    rows, cl = own.shape
+    fold = pieces[0].shape[0] - hd
+    cols = rows // fold
+    cw = cl // cols
+    early = cl - cw
+    if early:
+        mixed_ref[:, :early] = own[:, :early].astype(mixed_ref.dtype)
+    for c in range(cols):
+        part = slice(c * fold, (c + 1) * fold)
+        total = own[part, early:]
+        for k in range(1, n):
+            total = total + pieces[k][hd:, c * cw : (c + 1) * cw].astype(jnp.float32)
+        mixed_ref[part, early:] = total.astype(mixed_ref.dtype)
+    for c in copies:
+        c.wait()
+
+
+def finish_call(n, hd, own, sent, moved):
+    vmem = pl.BlockSpec(memory_space=pltpu.VMEM)
     return pl.pallas_call(
-        write,
-        out_shape=tuple(jax.ShapeDtypeStruct(s, t) for s, t in outs),
-        in_specs=[pl.BlockSpec(memory_space=vm)] * len(outs),
-        out_specs=(hbm,) * len(outs),
-        scratch_shapes=[dma((len(outs),))],
-        compiler_params=pltpu.CompilerParams(vmem_limit_bytes=1024 * 1024),
-        cost_estimate=pl.CostEstimate(flops=0, bytes_accessed=pinned, transcendentals=0),
-    )(*results)
+        functools.partial(finish_kernel, n, hd),
+        out_shape=(
+            jax.ShapeDtypeStruct(own.shape, jnp.bfloat16),
+            jax.ShapeDtypeStruct((n * hd, own.shape[1]), jnp.bfloat16),
+        ),
+        in_specs=[vmem] * (n + 1),
+        out_specs=(vmem, pl.BlockSpec(memory_space=pltpu.HBM)),
+        scratch_shapes=[pltpu.SemaphoreType.DMA((n,))],
+        compiler_params=pltpu.CompilerParams(vmem_limit_bytes=4 * 1024 * 1024),
+    )(own, sent, *moved)
 
 
 def body(

time: 320 us -> 313 us (0.978)
  Pallas kernels: 319 us -> 308 us
  starting transfers between devices: 0 us -> 3.55 us
    pallas_call x1, Pallas kernels: 310 us -> 297 us  [moe_call(): pl.pallas_call(functools.partial(moe_kernel, (n, ntp, group, slots, cols,...]
    ppermute x0 -> x3, starting transfers between devices: none -> 3.55 us  [moe_call(): lax.ppermute(sent[k - 1], 'fs', mate_pairs(k, n))]
  transfers between devices with their start and end apart: 0 -> 3, of which waited for: 0 -> 1; matrix products, arithmetic and copies ran while one was open for 0% -> 0% of each run, Pallas kernels for 0% -> 3%
where the time goes in v1:
time: 313 us
  Pallas kernels  308 us (98%)
  starting transfers between devices  3.55 us (1%)
    pallas_call x1, Pallas kernels, moe_call(): pl.pallas_call(functools.partial(moe_kernel, (n, ntp, group, slots, cols,...  297 us
    pallas_call x1, Pallas kernels, moe_call(): pl.pallas_call(write, out_shape=tuple((jax.ShapeDtypeStruct(s, t) for s,...  8.79 us
  transfers between devices with their start and end apart: 3, of which 1 were waited for; matrix products, arithmetic and copies ran while one was open for 0% of the time, Pallas kernels for 3%

profile of v1, /device:TPU:0, one launch (start us, length us, event | category | flops | bytes accessed | tf_op | source)
XLA Modules:
  0.0 312.8 jit_solution(17811628961979098750)
XLA Ops:
  0.6 297.3 %shard_map.153 = (bf16[16,64,4096]{2,1,0:T(8,128)(2,1)S(1)}, bf16[16,64,4096]{2,1,0:T(8,128)(2,1)S(1)}, bf16[16,512,512]{2,1,0:T(8,128)(2,1)S(1)}, bf16[64,4096]...) custom-call(s32[8,128]{1,0:T(8,128)} %bitcast.3, ...), custom_call_target="tpu_custom_call" | custom-call | flops 12884901888 | bytes 167772160 | tf_op jit(solution)/shard_map/pallas_call | solution.py:583
  297.9 0.8 collective-permute-start.1
  298.7 1.8 collective-permute-start.2
  300.5 1.0 collective-permute-start
  301.5 8.8 %shard_map.155 = (bf16[16,64,4096]{2,1,0:T(8,128)(2,1)}, bf16[16,64,4096]{2,1,0:T(8,128)(2,1)}, bf16[16,512,512]{2,1,0:T(8,128)(2,1)}, bf16[64,4096]{1,0:T(8,128)(2,1)}, bf16[64,4096]{1,0:T(8,128)(2,1)}) custom-call(bf16[16,64,4096]{2,1,0:T(8,128)(2,1)S(1)} %get-tuple-element.28.refs_0_, bf16[16,64,4096]{2,1,0:T(8,128)(2,1)S(1)} %get-tuple-element.29.refs_1_, ...), custom_call_target="tpu_custom_call" | custom-call | bytes 270663680 | tf_op jit(solution)/shard_map/pallas_call | solution.py:651
  310.3 0.0 collective-permute-done.1.refs_2_
  310.3 0.0 collective-permute-done.2.refs_3_
  310.3 1.1 collective-permute-done.refs_1_
  311.4 1.5 shard_map.154
Async XLA Ops:
  297.9 12.4 %collective-permute-start.1 = (bf16[192,512]{1,0:T(8,128)(2,1)S(1)}, bf16[192,512]{1,0:T(8,128)(2,1)S(1)}, u32[]{:S(2)}, u32[]{:S(2)}) collective-permute-start(bf16[192,512]{1,0:T(8,128)(2,1)S(1)} %get-tuple-element.25), channel_id=1, source_target_pairs={{0,16},{8,24},{16,0},{24,8},{1,17},{9,25},{17,1},{25,9},{2,18},{10... | collective-permute-start | bytes 589832 | tf_op jit(solution)/shard_map/ppermute | solution.py:650
  298.7 11.6 %collective-permute-start.2 = (bf16[192,512]{1,0:T(8,128)(2,1)S(1)}, bf16[192,512]{1,0:T(8,128)(2,1)S(1)}, u32[]{:S(2)}, u32[]{:S(2)}) collective-permute-start(bf16[192,512]{1,0:T(8,128)(2,1)S(1)} %get-tuple-element.26), channel_id=1, source_target_pairs={{0,24},{8,16},{16,8},{24,0},{1,25},{9,17},{17,9},{25,1},{2,26},{10... | collective-permute-start | bytes 589832 | tf_op jit(solution)/shard_map/ppermute | solution.py:650
  300.5 10.9 %collective-permute-start = (bf16[192,512]{1,0:T(8,128)(2,1)S(1)}, bf16[192,512]{1,0:T(8,128)(2,1)S(1)}, u32[]{:S(2)}, u32[]{:S(2)}) collective-permute-start(bf16[192,512]{1,0:T(8,128)(2,1)S(1)} %get-tuple-element.24.refs_0_), channel_id=1, source_target_pairs={{0,8},{8,0},{16,24},{24,16},{1,9},{9,1},{17,25},{25,17},{2,10},{10... | collective-permute-start | bytes 589832 | tf_op jit(solution)/shard_map/ppermute | solution.py:650

commit v2 on v1

--- a/solution.py
+++ b/solution.py
@@ -76,7 +76,7 @@
     cw = cl // cols
     neg = le // ge
     chunks = cols * neg
-    order = list(range(1, n)) + [0]
+    order = list(range(n - 1, -1, -1))
 
     def at(first, size):
         return pl.ds(pl.multiple_of(first, size), size)
@@ -106,12 +106,6 @@
 
     def own_tokens():
         return pltpu.make_async_copy(tok_ref, x.at[at(me * rows, rows), at(tp * cl, cl)], osem)
-
-    for i in range(len(early)):
-        early_load(i).start()
-    for k in order:
-        load(0, 0, k).start()
-    own_tokens().start()
 
     barrier = pltpu.get_barrier_semaphore()
     for k in range(1, n):
@@ -119,6 +113,21 @@
     for k in range(1, nz):
         pl.semaphore_signal(barrier, inc=1, device_id={"tp": zdest[k]}, device_id_type=MESH)
     pl.semaphore_signal(barrier, inc=1, device_id={"tp": partner}, device_id_type=MESH)
+    for i in range(len(early)):
+        early_load(i).start()
+    for k in order:
+        load(0, 0, k).start()
+    own_tokens().start()
+
+    for i in range(3):
+        early_load(i).wait()
+    affinity = affv[...]
+    route = jnp.concatenate(
+        [idv[...].astype(jnp.float32), routed_scale * affinity / jnp.sum(affinity, axis=0, keepdims=True)], axis=0
+    )
+    rbuf[...] = route
+    rland[me] = route
+    own_tokens().wait()
     pl.semaphore_wait(barrier, n - 1 + nz)
 
     relay = n == 4
@@ -182,16 +191,7 @@
             device_id_type=MESH,
         )
 
-    gather_start(tok_ref, token_place, token_sems)
-
-    for i in range(3):
-        early_load(i).wait()
-    affinity = affv[...]
-    route = jnp.concatenate(
-        [idv[...].astype(jnp.float32), routed_scale * affinity / jnp.sum(affinity, axis=0, keepdims=True)], axis=0
-    )
-    rbuf[...] = route
-    rland[me] = route
+    gather_start(token_place(me, None), token_place, token_sems)
 
     def weight_copy(w, k, slot, j, source):
         return pltpu.make_async_remote_copy(
@@ -292,7 +292,6 @@
     def token_view(slot):
         return x.at[:, at(slot * cl, cl)]
 
-    own_tokens().wait()
     gather_wait(token_place, token_sems)
     z_send(token_view, pick(zs), pick(zr))
     for k in range(1, n):
@@ -567,7 +566,7 @@
     le, d, hidden, total = experts // n, dl * n, hd * n, rows * n
     group = min(le, max(1, 128 // hl))
     pairs = le // group
-    slots = min(4, pairs)
+    slots = min(6, pairs)
     cols = 2 if cl % 256 == 0 else 1
     cw, early = cl // cols, max(1, cols - 1)
     ge = group * (2 if pairs % 2 == 0 else 1)

time: 313 us -> 312 us (level)
  no operation moved by 1% of the time
where the time goes in v2:
time: 312 us; the launch traced here: 311 us
  Pallas kernels  306 us (98%)
  starting transfers between devices  3.66 us (1%)
    pallas_call x1, Pallas kernels, moe_call(): pl.pallas_call(functools.partial(moe_kernel, (n, ntp, group, slots, cols,...  296 us
    pallas_call x1, Pallas kernels, moe_call(): pl.pallas_call(write, out_shape=tuple((jax.ShapeDtypeStruct(s, t) for s,...  8.79 us
  transfers between devices with their start and end apart: 3, of which 1 were waited for; matrix products, arithmetic and copies ran while one was open for 0% of the time, Pallas kernels for 3%

profile of v2, /device:TPU:0, one launch (start us, length us, event | category | flops | bytes accessed | tf_op | source)
XLA Modules:
  0.0 311.0 jit_solution(6157721805336160009)
XLA Ops:
  0.6 296.1 %shard_map.153 = (bf16[16,64,4096]{2,1,0:T(8,128)(2,1)S(1)}, bf16[16,64,4096]{2,1,0:T(8,128)(2,1)S(1)}, bf16[16,512,512]{2,1,0:T(8,128)(2,1)S(1)}, bf16[64,4096]...) custom-call(s32[8,128]{1,0:T(8,128)} %bitcast.3, ...), custom_call_target="tpu_custom_call" | custom-call | flops 12884901888 | bytes 167772160 | tf_op jit(solution)/shard_map/pallas_call | solution.py:582
  296.8 0.9 collective-permute-start.1
  297.7 2.7 collective-permute-start.2
  300.4 0.0 collective-permute-start
  300.4 8.8 %shard_map.155 = (bf16[16,64,4096]{2,1,0:T(8,128)(2,1)}, bf16[16,64,4096]{2,1,0:T(8,128)(2,1)}, bf16[16,512,512]{2,1,0:T(8,128)(2,1)}, bf16[64,4096]{1,0:T(8,128)(2,1)}, bf16[64,4096]{1,0:T(8,128)(2,1)}) custom-call(bf16[16,64,4096]{2,1,0:T(8,128)(2,1)S(1)} %get-tuple-element.28.refs_0_, bf16[16,64,4096]{2,1,0:T(8,128)(2,1)S(1)} %get-tuple-element.29.refs_1_, ...), custom_call_target="tpu_custom_call" | custom-call | bytes 270663680 | tf_op jit(solution)/shard_map/pallas_call | solution.py:650
  309.2 0.0 collective-permute-done.1.refs_2_
  309.3 0.0 collective-permute-done.2.refs_3_
  309.3 0.2 collective-permute-done.refs_1_
  309.5 1.5 shard_map.154
Async XLA Ops:
  296.8 12.5 %collective-permute-start.1 = (bf16[192,512]{1,0:T(8,128)(2,1)S(1)}, bf16[192,512]{1,0:T(8,128)(2,1)S(1)}, u32[]{:S(2)}, u32[]{:S(2)}) collective-permute-start(bf16[192,512]{1,0:T(8,128)(2,1)S(1)} %get-tuple-element.25), channel_id=1, source_target_pairs={{0,16},{8,24},{16,0},{24,8},{1,17},{9,25},{17,1},{25,9},{2,18},{10... | collective-permute-start | bytes 589832 | tf_op jit(solution)/shard_map/ppermute | solution.py:649
  297.7 11.6 %collective-permute-start.2 = (bf16[192,512]{1,0:T(8,128)(2,1)S(1)}, bf16[192,512]{1,0:T(8,128)(2,1)S(1)}, u32[]{:S(2)}, u32[]{:S(2)}) collective-permute-start(bf16[192,512]{1,0:T(8,128)(2,1)S(1)} %get-tuple-element.26), channel_id=1, source_target_pairs={{0,24},{8,16},{16,8},{24,0},{1,25},{9,17},{17,9},{25,1},{2,26},{10... | collective-permute-start | bytes 589832 | tf_op jit(solution)/shard_map/ppermute | solution.py:649
  300.4 9.1 %collective-permute-start = (bf16[192,512]{1,0:T(8,128)(2,1)S(1)}, bf16[192,512]{1,0:T(8,128)(2,1)S(1)}, u32[]{:S(2)}, u32[]{:S(2)}) collective-permute-start(bf16[192,512]{1,0:T(8,128)(2,1)S(1)} %get-tuple-element.24.refs_0_), channel_id=1, source_target_pairs={{0,8},{8,0},{16,24},{24,16},{1,9},{9,1},{17,25},{25,17},{2,10},{10... | collective-permute-start | bytes 589832 | tf_op jit(solution)/shard_map/ppermute | solution.py:649

commit v3 on v2

--- a/solution.py
+++ b/solution.py
@@ -30,6 +30,10 @@
 
 def mate_origin(me, k, n):
     return lax.rem(me + n - k, n) if n & (n - 1) else mate(me, k, n)
+
+
+def turn(k, n):
+    return k if n & (n - 1) else k ^ (k >> 1)
 
 
 def mate_pairs(k, n):
@@ -514,7 +518,7 @@
     lax.fori_loop(0, chunks, down_step, 0)
     fold = rows // cols
     for k in range(1, n):
-        to = mate(me, k, n)
+        to = mate(me, turn(k, n), n)
         lasts[k - 1][:hd, :] = ssb[...]
         for c in range(cols):
             lasts[k - 1][hd:, c * cw : (c + 1) * cw] = acc[at(to * rows + c * fold, fold), :].astype(jnp.bfloat16)
@@ -629,7 +633,7 @@
         cost_estimate=pl.CostEstimate(flops=6 * total * d * hl * le, bytes_accessed=40 * gate.size, transcendentals=0),
     )(*args)
 
-    cut = min(4, le)
+    cut = 1
 
     def write(*refs):
         count = len(serve)
@@ -646,7 +650,7 @@
             c.wait()
 
     own, sent = results[len(serve)], results[len(serve) + 1 :]
-    moved = [lax.ppermute(sent[k - 1], "fs", mate_pairs(k, n)) for k in range(1, n)]
+    moved = [lax.ppermute(sent[k - 1], "fs", mate_pairs(turn(k, n), n)) for k in range(1, n)]
     written = pl.pallas_call(
         write,
         out_shape=tuple(jax.ShapeDtypeStruct(s, t) for s, t in serve),
@@ -666,7 +670,7 @@
     me = lax.axis_index("fs")
     copies = []
     for k in range(n):
-        source = mate_origin(me, k, n)
+        source = mate_origin(me, turn(k, n), n)
         place = down_ref.at[pl.ds(pl.multiple_of(source * hd, hd), hd)]
         copies.append(pltpu.make_async_copy(pieces[k].at[pl.ds(0, hd)], place, sem.at[k]))
         copies[-1].start()

time: 312 us -> 312 us (level)
  no operation moved by 1% of the time
where the time goes in v3:
time: 312 us; the launch traced here: 311 us
  Pallas kernels  306 us (98%)
  starting transfers between devices  3.66 us (1%)
    pallas_call x1, Pallas kernels, moe_call(): pl.pallas_call(functools.partial(moe_kernel, (n, ntp, group, slots, cols,...  296 us
    pallas_call x1, Pallas kernels, moe_call(): pl.pallas_call(write, out_shape=tuple((jax.ShapeDtypeStruct(s, t) for s,...  8.8 us
  transfers between devices with their start and end apart: 3, of which 1 were waited for; matrix products, arithmetic and copies ran while one was open for 0% of the time, Pallas kernels for 3%

profile of v3, /device:TPU:0, one launch (start us, length us, event | category | flops | bytes accessed | tf_op | source)
XLA Modules:
  0.0 311.2 jit_solution(7651164569110582994)
XLA Ops:
  0.6 296.1 %shard_map.153 = (bf16[16,64,4096]{2,1,0:T(8,128)(2,1)S(1)}, bf16[16,64,4096]{2,1,0:T(8,128)(2,1)S(1)}, bf16[16,512,512]{2,1,0:T(8,128)(2,1)S(1)}, bf16[64,4096]...) custom-call(s32[8,128]{1,0:T(8,128)} %bitcast.3, ...), custom_call_target="tpu_custom_call" | custom-call | flops 12884901888 | bytes 167772160 | tf_op jit(solution)/shard_map/pallas_call | solution.py:586
  296.8 2.9 collective-permute-start.1
  299.7 0.7 collective-permute-start.2
  300.4 0.0 collective-permute-start
  300.4 8.8 %shard_map.155 = (bf16[16,64,4096]{2,1,0:T(8,128)(2,1)}, bf16[16,64,4096]{2,1,0:T(8,128)(2,1)}, bf16[16,512,512]{2,1,0:T(8,128)(2,1)}, bf16[64,4096]{1,0:T(8,128)(2,1)}, bf16[64,4096]{1,0:T(8,128)(2,1)}) custom-call(bf16[16,64,4096]{2,1,0:T(8,128)(2,1)S(1)} %get-tuple-element.28.refs_0_, bf16[16,64,4096]{2,1,0:T(8,128)(2,1)S(1)} %get-tuple-element.29.refs_1_, ...), custom_call_target="tpu_custom_call" | custom-call | bytes 270663680 | tf_op jit(solution)/shard_map/pallas_call | solution.py:654
  309.3 0.0 collective-permute-done.1.refs_2_
  309.3 0.4 collective-permute-done.2.refs_3_
  309.7 0.0 collective-permute-done.refs_1_
  309.7 1.5 shard_map.154
Async XLA Ops:
  296.8 12.5 %collective-permute-start.1 = (bf16[192,512]{1,0:T(8,128)(2,1)S(1)}, bf16[192,512]{1,0:T(8,128)(2,1)S(1)}, u32[]{:S(2)}, u32[]{:S(2)}) collective-permute-start(bf16[192,512]{1,0:T(8,128)(2,1)S(1)} %get-tuple-element.25), channel_id=1, source_target_pairs={{0,24},{8,16},{16,8},{24,0},{1,25},{9,17},{17,9},{25,1},{2,26},{10... | collective-permute-start | bytes 589832 | tf_op jit(solution)/shard_map/ppermute | solution.py:653
  299.7 10.0 %collective-permute-start.2 = (bf16[192,512]{1,0:T(8,128)(2,1)S(1)}, bf16[192,512]{1,0:T(8,128)(2,1)S(1)}, u32[]{:S(2)}, u32[]{:S(2)}) collective-permute-start(bf16[192,512]{1,0:T(8,128)(2,1)S(1)} %get-tuple-element.26), channel_id=1, source_target_pairs={{0,16},{8,24},{16,0},{24,8},{1,17},{9,25},{17,1},{25,9},{2,18},{10... | collective-permute-start | bytes 589832 | tf_op jit(solution)/shard_map/ppermute | solution.py:653
  300.4 9.3 %collective-permute-start = (bf16[192,512]{1,0:T(8,128)(2,1)S(1)}, bf16[192,512]{1,0:T(8,128)(2,1)S(1)}, u32[]{:S(2)}, u32[]{:S(2)}) collective-permute-start(bf16[192,512]{1,0:T(8,128)(2,1)S(1)} %get-tuple-element.24.refs_0_), channel_id=1, source_target_pairs={{0,8},{8,0},{16,24},{24,16},{1,9},{9,1},{17,25},{25,17},{2,10},{10... | collective-permute-start | bytes 589832 | tf_op jit(solution)/shard_map/ppermute | solution.py:653
